TPU v7x, 32 devices: a whole 2x2x4 slice. The times are simulated.
32 devices in a mesh: tp: 16 (over z, y, x), dp: 2 (over core).
Axes of the slice: x: 2, y: 2, z: 4, core: 2. Of those that a mesh axis runs over, the one named last changes fastest.
Arguments:
- tokens: bfloat16 [256, 4096], P(None, 'dp'), may hold values from -20 to 20
- norm_gain: float32 [2, 4096], P(None, 'dp'), may hold values from 0.1 to 1.9
- receptance: bfloat16 [2, 4096, 1024], P(None, 'dp', 'tp'), may hold values from -0.09375 to 0.09375
- key_proj: bfloat16 [2, 4096, 1024], P(None, 'dp', 'tp'), may hold values from -0.09375 to 0.09375
- value_proj: bfloat16 [2, 4096, 1024], P(None, 'dp', 'tp'), may hold values from -0.09375 to 0.09375
- decay_proj: bfloat16 [2, 4096, 1024], P(None, 'dp', 'tp'), may hold values from -0.09375 to 0.09375
- rate_proj: bfloat16 [2, 4096, 1024], P(None, 'dp', 'tp'), may hold values from -0.09375 to 0.09375
- gate_proj: bfloat16 [2, 4096, 1024], P(None, 'dp', 'tp'), may hold values from -0.09375 to 0.09375
- decay_base: float32 [2, 1024], P(None, 'tp'), may hold values from -6 to 1
- group_gain: float32 [2, 1024], P(None, 'tp'), may hold values from 0.1 to 1.9
- output_proj: bfloat16 [2, 1024, 4096], P(None, 'tp', 'dp'), may hold values from -0.1875 to 0.1875
- state: float32 [2, 256, 16, 4096], P(None, 'dp', 'tp'), may hold values from -3 to 3
Outputs:
- next_tokens: bfloat16 [256, 4096], P(None, 'dp')
- new_state: float32 [2, 256, 16, 4096], P(None, 'dp', 'tp')
All inputs are finite; a program needn't handle non-finite values.
Results may differ from a plain program's by a relative error of at most 0.0066.
Values may be sent and summed in bfloat16 or wider, within the bound.
No kernel may reach another device: no remote copies, remote signals or barrier semaphores. Data moves between devices by JAX's collectives and lax.ppermute only.
A program may use at most 64 MiB of HBM per device.

v0:
```python
import jax
import jax.numpy as jnp
from jax import lax
from jax.sharding import PartitionSpec as P

D = 4096
HEAD = 64
LAYERS = 2
norm_floor = 0.1
group_floor = 0.5


def recurrence(state_block, recept_heads, key_heads, value_heads, decay_heads, rate_heads):
    log_rate = -jax.nn.softplus(-decay_heads) - 0.5
    forget = jnp.exp(-jnp.exp(log_rate))
    learn_rate = jax.nn.sigmoid(rate_heads)
    unit_key = key_heads * lax.rsqrt(jnp.sum(key_heads * key_heads, axis=-1, keepdims=True) + 1.0)
    scaled = key_heads * learn_rate
    removed = jnp.einsum("bhvk,bhk->bhv", state_block, -unit_key, precision=lax.Precision.HIGHEST)
    updated = (
        state_block * forget[:, :, None, :]
        + removed[..., None] * (unit_key * learn_rate)[:, :, None, :]
        + value_heads[..., None] * scaled[:, :, None, :]
    )
    read_out = jnp.einsum("bhvk,bhk->bhv", updated, recept_heads, precision=lax.Precision.HIGHEST)
    centre = read_out - jnp.mean(read_out, axis=-1, keepdims=True)
    normal = centre * lax.rsqrt(jnp.mean(centre * centre, axis=-1, keepdims=True) + group_floor)
    return (updated, normal)


def shards(
    tokens,
    norm_gain,
    receptance,
    key_proj,
    value_proj,
    decay_proj,
    rate_proj,
    gate_proj,
    decay_base,
    group_gain,
    output_proj,
    state,
):
    local_rows = state.shape[1]
    first_row = lax.axis_index("dp") * local_rows
    local_heads = state.shape[2]
    current = tokens
    finals = []
    for section_index in range(LAYERS):
        floats = current.astype(jnp.float32)
        squares = jnp.sum(floats * floats, axis=1)
        normed = (floats * norm_gain[section_index]).astype(jnp.bfloat16)
        part_recept = jnp.dot(normed, receptance[section_index], preferred_element_type=jnp.float32)
        part_key = jnp.dot(normed, key_proj[section_index], preferred_element_type=jnp.float32)
        part_value = jnp.dot(normed, value_proj[section_index], preferred_element_type=jnp.float32)
        part_decay = jnp.dot(normed, decay_proj[section_index], preferred_element_type=jnp.float32)
        part_rate = jnp.dot(normed, rate_proj[section_index], preferred_element_type=jnp.float32)
        part_gate = jnp.dot(normed, gate_proj[section_index], preferred_element_type=jnp.float32)
        totals = lax.psum(squares, "dp")
        own_squares = lax.dynamic_slice_in_dim(totals, first_row, local_rows, 0)
        summed = (
            lax.psum_scatter(part_recept, "dp", scatter_dimension=0, tiled=True),
            lax.psum_scatter(part_key, "dp", scatter_dimension=0, tiled=True),
            lax.psum_scatter(part_value, "dp", scatter_dimension=0, tiled=True),
            lax.psum_scatter(part_decay, "dp", scatter_dimension=0, tiled=True),
            lax.psum_scatter(part_rate, "dp", scatter_dimension=0, tiled=True),
            lax.psum_scatter(part_gate, "dp", scatter_dimension=0, tiled=True),
        )
        inv_rms = lax.rsqrt(own_squares / D + norm_floor)

        def by_head(term):
            rounded = lax.optimization_barrier((inv_rms[:, None] * term).astype(jnp.bfloat16))
            return rounded.astype(jnp.float32).reshape(local_rows, local_heads, HEAD)

        decay_heads = by_head(summed[3]) + decay_base[section_index].reshape(1, local_heads, HEAD)
        updated, normal = recurrence(
            state[section_index].reshape(local_rows, local_heads, HEAD, HEAD),
            by_head(summed[0]),
            by_head(summed[1]),
            by_head(summed[2]),
            decay_heads,
            by_head(summed[4]),
        )
        finals.append(updated.reshape(local_rows, local_heads, HEAD * HEAD))
        gate_value = jax.nn.sigmoid(by_head(summed[5]).reshape(local_rows, local_heads * HEAD))
        mixed_heads = (
            normal.reshape(local_rows, local_heads * HEAD) * group_gain[section_index] * gate_value
        ).astype(jnp.bfloat16)
        weights_out = output_proj[section_index]

        def apply_out(piece, begin, weights_out=weights_out):
            return jnp.dot(piece, weights_out, preferred_element_type=jnp.float32)

        partial_out = apply_out(lax.all_gather(mixed_heads, "dp", axis=0, tiled=True), jnp.int32(0))
        total = lax.psum(partial_out, "tp")
        current = (floats + total).astype(jnp.bfloat16)
    return (current, jnp.stack(finals))


def solution(mesh):
    return jax.shard_map(
        shards,
        mesh=mesh,
        in_specs=(
            P(None, "dp"),
            P(None, "dp"),
            P(None, "dp", "tp"),
            P(None, "dp", "tp"),
            P(None, "dp", "tp"),
            P(None, "dp", "tp"),
            P(None, "dp", "tp"),
            P(None, "dp", "tp"),
            P(None, "tp"),
            P(None, "tp"),
            P(None, "tp", "dp"),
            P(None, "dp", "tp", None),
        ),
        out_specs=(P(None, "dp"), P(None, "dp", "tp", None)),
        check_vma=False,
    )
```

profile of v0, /device:TPU:0, one launch (start us, length us, event | category | flops | bytes accessed | tf_op | source)
XLA Modules:
  0.0 421.7 jit_solution(14630838087907600654)
XLA Ops:
  7.2 0.9 fusion.78
  8.1 2.3 fusion.22
  10.5 2.4 fusion.26
  13.0 1.1 fusion.24
  14.1 1.1 fusion.20
  15.3 1.1 fusion.18
  16.5 1.1 fusion.28
  17.6 8.1 %fusion.77 = (f32[1,128,1,4096]{3,2,1,0:T(1,128)}, f32[1,128,1,4096]{3,2,1,0:T(1,128)}) fusion(f32[2,128,1,4096]{3,2,1,0:T(1,128)} %param.23), kind=kLoop, calls=%fused_computation.119 | loop fusion | bytes 8388608 | tf_op jit(solution)/shard_map/slice | solution.py:78
  26.0 5.0 %copy.45 = f32[1,128,1,4096]{1,3,2,0:T(8,128)S(1)} copy(f32[1,128,1,4096]{3,2,1,0:T(1,128)} %get-tuple-element.7) | data formatting | bytes 4194304
  31.1 2.6 psum.28
  33.8 9.1 %reduce-scatter.17.cloned.1.call-done = f32[128,64]{0,1:T(8,128)} async-done(((f32[256,64]{0,1:T(8,128)}), f32[128,64]{0,1:T(8,128)}) %reduce-scatter.17.cloned.1.call-update) | async-done | bytes 32784 | tf_op jit(solution)/shard_map/reduce_scatter | solution.py:67
  42.8 10.7 %reduce-scatter.21.cloned.1.call-done = f32[128,64]{0,1:T(8,128)} async-done(((f32[256,64]{0,1:T(8,128)}), f32[128,64]{0,1:T(8,128)}) %reduce-scatter.21.cloned.1.call-update) | async-done | bytes 32784 | tf_op jit(solution)/shard_map/reduce_scatter | solution.py:63
  53.6 10.7 %reduce-scatter.23.cloned.1.call-done = f32[128,64]{0,1:T(8,128)} async-done(((f32[256,64]{0,1:T(8,128)}), f32[128,64]{0,1:T(8,128)}) %reduce-scatter.23.cloned.1.call-update) | async-done | bytes 32784 | tf_op jit(solution)/shard_map/reduce_scatter | solution.py:68
  64.3 10.7 %reduce-scatter.13.cloned.1.call-done = f32[128,64]{0,1:T(8,128)} async-done(((f32[256,64]{0,1:T(8,128)}), f32[128,64]{0,1:T(8,128)}) %reduce-scatter.13.cloned.1.call-update) | async-done | bytes 32784 | tf_op jit(solution)/shard_map/reduce_scatter | solution.py:66
  75.1 0.9 multiply_convert_fusion.10
  76.5 0.7 multiply_reduce_fusion.2
  77.4 1.9 all_gather.6
  79.2 2.7 fusion.38
  82.0 5.6 %copy.46 = f32[1,128,1,4096]{1,3,2,0:T(8,128)} copy(f32[1,128,1,4096]{3,2,1,0:T(1,128)} %get-tuple-element.6) | data formatting | bytes 4194304
  87.7 122.2 %all-reduce.3.cloned.1.call-done = f32[256,2048]{1,0:T(8,128)} async-done(((f32[256,2048]{1,0:T(8,128)}), f32[256,2048]{1,0:T(8,128)}) %all-reduce.3.cloned.1.call-update) | async-done | bytes 2097168 | tf_op jit(solution)/shard_map/psum | solution.py:96
  209.9 2.0 fusion.3
  211.9 1.0 copy-done.4
  212.9 1.1 fusion.10
  214.0 2.4 fusion.14
  216.5 2.3 fusion.12
  218.9 2.0 fusion.8
  221.1 2.0 fusion.6
  223.1 2.0 fusion.16
  225.2 2.6 broadcast_multiply_fusion.2
  227.8 2.6 psum.30
  230.5 1.3 reduce-scatter.27.cloned.1.call-done
  231.9 10.7 %reduce-scatter.29.cloned.1.call-done = f32[128,64]{0,1:T(8,128)} async-done(((f32[256,64]{0,1:T(8,128)}), f32[128,64]{0,1:T(8,128)}) %reduce-scatter.29.cloned.1.call-update) | async-done | bytes 32784 | tf_op jit(solution)/shard_map/reduce_scatter | solution.py:67
  242.6 11.5 %reduce-scatter.33.cloned.1.call-done = f32[128,64]{0,1:T(8,128)} async-done(((f32[256,64]{0,1:T(8,128)}), f32[128,64]{0,1:T(8,128)}) %reduce-scatter.33.cloned.1.call-update) | async-done | bytes 32784 | tf_op jit(solution)/shard_map/reduce_scatter | solution.py:63
  254.1 10.7 %reduce-scatter.35.cloned.1.call-done = f32[128,64]{0,1:T(8,128)} async-done(((f32[256,64]{0,1:T(8,128)}), f32[128,64]{0,1:T(8,128)}) %reduce-scatter.35.cloned.1.call-update) | async-done | bytes 32784 | tf_op jit(solution)/shard_map/reduce_scatter | solution.py:68
  264.8 10.9 %reduce-scatter.25.cloned.1.call-done = f32[128,64]{0,1:T(8,128)} async-done(((f32[256,64]{0,1:T(8,128)}), f32[128,64]{0,1:T(8,128)}) %reduce-scatter.25.cloned.1.call-update) | async-done | bytes 32784 | tf_op jit(solution)/shard_map/reduce_scatter | solution.py:66
  275.7 1.0 multiply_convert_fusion.3
  276.9 1.9 multiply_reduce_fusion.1
  278.9 0.8 multiply_reduce_fusion
  279.8 1.9 all_gather.7
  281.7 2.7 fusion.30
  284.7 1.3 copy-done.2
  286.0 2.1 add_add_fusion.1
  288.8 1.3 copy-done.1
  290.1 0.6 add_add_fusion
  290.8 2.2 pad_maximum_fusion
  292.9 10.1 %copy.24 = f32[2,128,1,4096]{3,2,1,0:T(1,128)} copy(f32[2,128,1,4096]{1,3,2,0:T(8,128)} %pad_maximum_fusion) | data formatting | bytes 8388608
  303.1 109.3 %all-reduce.5.cloned.1.call-done = f32[256,2048]{1,0:T(8,128)} async-done(((f32[256,2048]{1,0:T(8,128)}), f32[256,2048]{1,0:T(8,128)}) %all-reduce.5.cloned.1.call-update) | async-done | bytes 2097168 | tf_op jit(solution)/shard_map/psum | solution.py:96
  412.4 2.8 fusion.5
  (85 shorter events, 3.2 us)
Async XLA Ops:
  7.2 5.8 %copy-start.3 = (bf16[256,2048]{1,0:T(8,128)(2,1)S(1)}, bf16[256,2048]{1,0:T(8,128)(2,1)}, u32[]{:S(2)}) copy-start(bf16[256,2048]{1,0:T(8,128)(2,1)} %param.12) | copy-start | bytes 3145732
  7.2 5.8 %copy-start.9 = (bf16[2,2048,64]{1,2,0:T(8,128)(2,1)S(1)}, bf16[2,2048,64]{1,2,0:T(8,128)(2,1)}, u32[]{:S(2)}) copy-start(bf16[2,2048,64]{1,2,0:T(8,128)(2,1)} %param.18) | copy-start | bytes 1572868
  7.2 26.6 %reduce-scatter.19.cloned.1.call-start = ((), (), s32[]{:S(2)}) async-start(), calls=%async_computation.15 | async-start | bytes 98304 | tf_op jit(solution)/shard_map/reduce_scatter | solution.py:65
  10.4 3.7 copy-start.10
  10.5 23.3 %reduce-scatter.15.cloned.1.call-start = ((), (), s32[]{:S(2)}) async-start(), calls=%async_computation.13 | async-start | bytes 98304 | tf_op jit(solution)/shard_map/reduce_scatter | solution.py:64
  12.9 2.4 copy-start.11
  12.9 29.9 %reduce-scatter.17.cloned.1.call-start = ((), (), s32[]{:S(2)}) async-start(), calls=%async_computation.14 | async-start | bytes 98304 | tf_op jit(solution)/shard_map/reduce_scatter | solution.py:67
  14.1 2.4 copy-start.12
  14.1 39.5 %reduce-scatter.21.cloned.1.call-start = ((), (), s32[]{:S(2)}) async-start(), calls=%async_computation.16 | async-start | bytes 98304 | tf_op jit(solution)/shard_map/reduce_scatter | solution.py:63
  15.2 49.1 %reduce-scatter.23.cloned.1.call-start = ((), (), s32[]{:S(2)}) async-start(), calls=%async_computation.17 | async-start | bytes 98304 | tf_op jit(solution)/shard_map/reduce_scatter | solution.py:68
  16.4 58.7 %reduce-scatter.13.cloned.1.call-start = ((), (), s32[]{:S(2)}) async-start(), calls=%async_computation.12 | async-start | bytes 98304 | tf_op jit(solution)/shard_map/reduce_scatter | solution.py:66
  17.5 8.2 %copy-start.6 = (f32[2,64]{1,0:T(2,128)S(1)}, f32[2,64]{1,0:T(2,128)}, u32[]{:S(2)}) copy-start(f32[2,64]{1,0:T(2,128)} %param.20) | copy-start | bytes 1540
  17.6 8.1 %copy-start.7 = (f32[2,64]{1,0:T(2,128)S(1)}, f32[2,64]{1,0:T(2,128)}, u32[]{:S(2)}) copy-start(f32[2,64]{1,0:T(2,128)} %param.21) | copy-start | bytes 1540
  17.6 192.3 %all-reduce.3.cloned.1.call-start = ((), (), s32[]{:S(2)}) async-start(), calls=%async_computation.18 | async-start | bytes 4194304 | tf_op jit(solution)/shard_map/psum | solution.py:96
  82.0 148.6 %reduce-scatter.31.cloned.1.call-start = ((), (), s32[]{:S(2)}) async-start(), calls=%async_computation.22 | async-start | bytes 98304 | tf_op jit(solution)/shard_map/reduce_scatter | solution.py:65
  209.9 3.0 copy-start.8
  211.9 1.0 copy-start.4
  214.0 5.0 %copy-start.5 = (bf16[256,2048]{1,0:T(8,128)(2,1)S(1)}, bf16[256,2048]{1,0:T(8,128)(2,1)}, u32[]{:S(2)}) copy-start(bf16[256,2048]{1,0:T(8,128)(2,1)} %copy-done.4) | copy-start | bytes 3145732
  214.0 17.9 %reduce-scatter.27.cloned.1.call-start = ((), (), s32[]{:S(2)}) async-start(), calls=%async_computation.20 | async-start | bytes 98304 | tf_op jit(solution)/shard_map/reduce_scatter | solution.py:64
  216.5 26.1 %reduce-scatter.29.cloned.1.call-start = ((), (), s32[]{:S(2)}) async-start(), calls=%async_computation.21 | async-start | bytes 98304 | tf_op jit(solution)/shard_map/reduce_scatter | solution.py:67
  218.9 35.2 %reduce-scatter.33.cloned.1.call-start = ((), (), s32[]{:S(2)}) async-start(), calls=%async_computation.23 | async-start | bytes 98304 | tf_op jit(solution)/shard_map/reduce_scatter | solution.py:63
  221.0 43.8 %reduce-scatter.35.cloned.1.call-start = ((), (), s32[]{:S(2)}) async-start(), calls=%async_computation.24 | async-start | bytes 98304 | tf_op jit(solution)/shard_map/reduce_scatter | solution.py:68
  223.1 52.6 %reduce-scatter.25.cloned.1.call-start = ((), (), s32[]{:S(2)}) async-start(), calls=%async_computation.19 | async-start | bytes 98304 | tf_op jit(solution)/shard_map/reduce_scatter | solution.py:66
  225.2 187.2 %all-reduce.5.cloned.1.call-start = ((), (), s32[]{:S(2)}) async-start(), calls=%async_computation.25 | async-start | bytes 4194304 | tf_op jit(solution)/shard_map/psum | solution.py:96
  275.7 3.2 copy-start
  284.4 1.6 copy-start.2
  288.5 1.6 copy-start.1
Sparse Core Ops, SparseCore 0:
  10.8 10.2 reduce-scatter.18
  23.2 8.6 reduce-scatter.14
  34.2 8.6 reduce-scatter.16
  44.9 8.6 reduce-scatter.20
  55.6 8.6 reduce-scatter.22
  66.4 8.6 reduce-scatter.12
  82.1 127.7 all-reduce.2
  214.1 6.7 reduce-scatter.30
  223.1 8.7 reduce-scatter.26
  233.9 8.6 reduce-scatter.28
  245.4 8.6 reduce-scatter.32
  256.1 8.6 reduce-scatter.34
  267.0 8.6 reduce-scatter.24
  284.6 127.7 all-reduce.4
where the time goes:
time: 423 us; the launch traced here: 422 us
  waiting for transfers between devices  318 us (75%)
  local copies, waits for them, and re-layouts  33.9 us (8%)
  matrix products  26.4 us (6%)
  other arithmetic  19.5 us (5%)
  between operations  14.2 us (3%)
  blocking collectives  8.96 us (2%)
    psum x2, waiting for transfers between devices, shards(): total = lax.psum(partial_out, 'tp')  231 us
    unnamed x29, local copies, waits for them, and re-layouts  24.5 us
    reduce_scatter x2, waiting for transfers between devices, shards(): lax.psum_scatter(part_recept, 'dp', scatter_dimension=0, tiled=True)  22.2 us
    reduce_scatter x2, waiting for transfers between devices, shards(): lax.psum_scatter(part_decay, 'dp', scatter_dimension=0, tiled=True)  21.6 us
    reduce_scatter x2, waiting for transfers between devices, shards(): lax.psum_scatter(part_gate, 'dp', scatter_dimension=0, tiled=True)  21.5 us
    reduce_scatter x2, waiting for transfers between devices, shards(): lax.psum_scatter(part_rate, 'dp', scatter_dimension=0, tiled=True)  19.8 us
  transfers between devices with their start and end apart: 14, of which 11 were waited for; matrix products, arithmetic and copies ran while one was open for 13% of the time, Pallas kernels for 0%

commit v1 on v0

--- a/solution.py
+++ b/solution.py
@@ -93,7 +93,8 @@
             return jnp.dot(piece, weights_out, preferred_element_type=jnp.float32)
 
         partial_out = apply_out(lax.all_gather(mixed_heads, "dp", axis=0, tiled=True), jnp.int32(0))
-        total = lax.psum(partial_out, "tp")
+        terms = lax.all_gather(partial_out, "tp", axis=0, tiled=False)
+        total = terms.sum(axis=0)
         current = (floats + total).astype(jnp.bfloat16)
     return (current, jnp.stack(finals))
 

time: 423 us -> 893 us (2.11)
  waiting for transfers between devices: 318 us -> 769 us
  other arithmetic: 19.5 us -> 39.2 us
    all_gather x0 -> x2, waiting for transfers between devices: none -> 687 us  [shards(): terms = lax.all_gather(partial_out, 'tp', axis=0, tiled=False)]
    psum x2 -> x0, waiting for transfers between devices: 231 us -> none  [shards(): total = lax.psum(partial_out, 'tp')]
    reduce_sum x0 -> x2, other arithmetic: none -> 24.9 us  [shards(): total = terms.sum(axis=0)]
    reduce_scatter x2, waiting for transfers between devices: 0.01 us -> 22.8 us  [shards(): lax.psum_scatter(part_value, 'dp', scatter_dimension=0, tiled=True)]
    reduce_scatter x2, waiting for transfers between devices: 21.6 us -> 0.01 us  [shards(): lax.psum_scatter(part_decay, 'dp', scatter_dimension=0, tiled=True)]
    unnamed x29 -> x27, local copies, waits for them, and re-layouts: 24.5 us -> 23.4 us
  transfers between devices with their start and end apart: 14 -> 14, of which waited for: 11 -> 10; matrix products, arithmetic and copies ran while one was open for 13% -> 6% of each run, Pallas kernels for 0% -> 0%
where the time goes in v1:
time: 893 us; the launch traced here: 892 us
  waiting for transfers between devices  769 us (86%)
  other arithmetic  39.2 us (4%)
  local copies, waits for them, and re-layouts  32.8 us (4%)
  matrix products  26.3 us (3%)
  between operations  14.2 us (2%)
  blocking collectives  8.96 us (1%)
    all_gather x2, waiting for transfers between devices, shards(): terms = lax.all_gather(partial_out, 'tp', axis=0, tiled=False)  687 us
    reduce_sum x2, other arithmetic, shards(): total = terms.sum(axis=0)  24.9 us
    unnamed x27, local copies, waits for them, and re-layouts  23.4 us
    reduce_scatter x2, waiting for transfers between devices, shards(): lax.psum_scatter(part_value, 'dp', scatter_dimension=0, tiled=True)  22.8 us
    reduce_scatter x2, waiting for transfers between devices, shards(): lax.psum_scatter(part_recept, 'dp', scatter_dimension=0, tiled=True)  21.6 us
    reduce_scatter x2, waiting for transfers between devices, shards(): lax.psum_scatter(part_gate, 'dp', scatter_dimension=0, tiled=True)  21.5 us
  transfers between devices with their start and end apart: 14, of which 10 were waited for; matrix products, arithmetic and copies ran while one was open for 6% of the time, Pallas kernels for 0%

profile of v1, /device:TPU:0, one launch (start us, length us, event | category | flops | bytes accessed | tf_op | source)
XLA Modules:
  0.0 891.5 jit_solution(6892970176508790689)
XLA Ops:
  7.2 0.9 fusion.78
  8.1 2.3 fusion.28
  10.5 2.4 fusion.26
  13.0 1.1 fusion.24
  14.1 1.1 fusion.22
  15.3 1.1 fusion.20
  16.5 1.1 fusion.18
  17.6 8.1 fusion.77
  26.0 5.0 copy.45
  31.1 2.6 psum.14
  33.8 8.9 reduce-scatter.17.cloned.1.call-done
  42.6 11.3 %reduce-scatter.19.cloned.1.call-done = f32[128,64]{0,1:T(8,128)} async-done(((f32[256,64]{0,1:T(8,128)}), f32[128,64]{0,1:T(8,128)}) %reduce-scatter.19.cloned.1.call-update) | async-done | bytes 32784 | tf_op jit(solution)/shard_map/reduce_scatter | solution.py:65
  54.0 10.7 %reduce-scatter.21.cloned.1.call-done = f32[128,64]{0,1:T(8,128)} async-done(((f32[256,64]{0,1:T(8,128)}), f32[128,64]{0,1:T(8,128)}) %reduce-scatter.21.cloned.1.call-update) | async-done | bytes 32784 | tf_op jit(solution)/shard_map/reduce_scatter | solution.py:63
  64.7 10.7 %reduce-scatter.23.cloned.1.call-done = f32[128,64]{0,1:T(8,128)} async-done(((f32[256,64]{0,1:T(8,128)}), f32[128,64]{0,1:T(8,128)}) %reduce-scatter.23.cloned.1.call-update) | async-done | bytes 32784 | tf_op jit(solution)/shard_map/reduce_scatter | solution.py:68
  75.4 0.9 multiply_convert_fusion.10
  76.8 0.7 multiply_reduce_fusion.2
  77.7 1.9 all_gather.18
  79.6 2.7 fusion.38
  82.4 351.5 %all-gather.5.cloned.1.call-done = f32[4096,2048]{1,0:T(8,128)} async-done(((f32[256,2048]{1,0:T(8,128)}), f32[4096,2048]{1,0:T(8,128)}) %all-gather.5.cloned.1.call-update) | async-done | bytes 33554448 | tf_op jit(solution)/shard_map/all_gather | solution.py:96
  433.9 13.1 %reduce_sum.94 = f32[256,2048]{1,0:T(8,128)} reduce(f32[16,256,2048]{2,1,0:T(8,128)} %bitcast.73, f32[]{:T(128)} %constant.11.clone.1), dimensions={0}, to_apply=%region_11.12 | reduce | flops 7864320 | bytes 35651588 | tf_op jit(solution)/shard_map/reduce_sum | solution.py:97
  447.0 2.0 fusion.3
  449.0 1.0 copy-done.3
  450.0 1.1 fusion.16
  451.1 2.4 fusion.14
  453.6 2.3 fusion.12
  456.1 2.0 fusion.8
  458.1 2.0 fusion.6
  460.2 2.0 fusion.10
  462.3 5.6 copy.46
  468.0 2.6 psum.15
  470.7 7.9 reduce-scatter.29.cloned.1.call-done
  478.6 10.9 %reduce-scatter.33.cloned.1.call-done = f32[128,64]{0,1:T(8,128)} async-done(((f32[256,64]{0,1:T(8,128)}), f32[128,64]{0,1:T(8,128)}) %reduce-scatter.33.cloned.1.call-update) | async-done | bytes 32784 | tf_op jit(solution)/shard_map/reduce_scatter | solution.py:63
  489.5 10.7 %reduce-scatter.35.cloned.1.call-done = f32[128,64]{0,1:T(8,128)} async-done(((f32[256,64]{0,1:T(8,128)}), f32[128,64]{0,1:T(8,128)}) %reduce-scatter.35.cloned.1.call-update) | async-done | bytes 32784 | tf_op jit(solution)/shard_map/reduce_scatter | solution.py:68
  500.2 11.5 %reduce-scatter.31.cloned.1.call-done = f32[128,64]{0,1:T(8,128)} async-done(((f32[256,64]{0,1:T(8,128)}), f32[128,64]{0,1:T(8,128)}) %reduce-scatter.31.cloned.1.call-update) | async-done | bytes 32784 | tf_op jit(solution)/shard_map/reduce_scatter | solution.py:65
  511.7 1.0 multiply_convert_fusion.3
  512.8 1.9 multiply_reduce_fusion.1
  514.8 0.8 multiply_reduce_fusion
  515.8 1.9 all_gather.21
  517.6 2.7 fusion.30
  520.4 0.6 broadcast_multiply_fusion.2
  521.2 0.4 add_add_fusion.1
  521.6 0.6 broadcast_multiply_fusion
  522.5 1.3 copy-done.1
  524.2 2.3 pad_maximum_fusion
  526.5 10.4 %copy.24 = f32[2,128,1,4096]{3,2,1,0:T(1,128)} copy(f32[2,128,1,4096]{1,3,2,0:T(8,128)} %pad_maximum_fusion) | data formatting | bytes 8388608
  536.9 335.1 %all-gather.7.cloned.1.call-done = f32[4096,2048]{1,0:T(8,128)} async-done(((f32[256,2048]{1,0:T(8,128)}), f32[4096,2048]{1,0:T(8,128)}) %all-gather.7.cloned.1.call-update) | async-done | bytes 33554448 | tf_op jit(solution)/shard_map/all_gather | solution.py:96
  871.9 11.8 %reduce_sum.99 = f32[256,2048]{1,0:T(8,128)S(1)} reduce(f32[16,256,2048]{2,1,0:T(8,128)} %bitcast.72, f32[]{:T(128)} %constant.11.clone.1), dimensions={0}, to_apply=%region_23.24 | reduce | flops 7864320 | bytes 35651588 | tf_op jit(solution)/shard_map/reduce_sum | solution.py:97
  883.7 1.3 fusion.5
  (85 shorter events, 3.2 us)
Async XLA Ops:
  7.2 5.8 copy-start.2
  7.2 5.8 copy-start.8
  7.2 26.6 %reduce-scatter.13.cloned.1.call-start = ((), (), s32[]{:S(2)}) async-start(), calls=%async_computation.12 | async-start | bytes 98304 | tf_op jit(solution)/shard_map/reduce_scatter | solution.py:66
  10.4 3.7 copy-start.11
  10.5 23.3 %reduce-scatter.15.cloned.1.call-start = ((), (), s32[]{:S(2)}) async-start(), calls=%async_computation.13 | async-start | bytes 98304 | tf_op jit(solution)/shard_map/reduce_scatter | solution.py:64
  12.9 2.4 copy-start.9
  12.9 29.7 %reduce-scatter.17.cloned.1.call-start = ((), (), s32[]{:S(2)}) async-start(), calls=%async_computation.14 | async-start | bytes 98304 | tf_op jit(solution)/shard_map/reduce_scatter | solution.py:67
  14.0 2.4 copy-start.10
  14.1 39.9 %reduce-scatter.19.cloned.1.call-start = ((), (), s32[]{:S(2)}) async-start(), calls=%async_computation.15 | async-start | bytes 98304 | tf_op jit(solution)/shard_map/reduce_scatter | solution.py:65
  15.2 49.4 %reduce-scatter.21.cloned.1.call-start = ((), (), s32[]{:S(2)}) async-start(), calls=%async_computation.16 | async-start | bytes 98304 | tf_op jit(solution)/shard_map/reduce_scatter | solution.py:63
  16.4 59.0 %reduce-scatter.23.cloned.1.call-start = ((), (), s32[]{:S(2)}) async-start(), calls=%async_computation.17 | async-start | bytes 98304 | tf_op jit(solution)/shard_map/reduce_scatter | solution.py:68
  17.5 8.2 copy-start.5
  17.6 8.2 copy-start.6
  17.6 416.3 %all-gather.5.cloned.1.call-start = ((), (), s32[]{:S(2)}) async-start(), calls=%async_computation.24 | async-start | bytes 35651584 | tf_op jit(solution)/shard_map/all_gather | solution.py:96
  82.3 388.4 %reduce-scatter.25.cloned.1.call-start = ((), (), s32[]{:S(2)}) async-start(), calls=%async_computation.18 | async-start | bytes 98304 | tf_op jit(solution)/shard_map/reduce_scatter | solution.py:66
  447.0 3.0 copy-start.7
  449.0 1.0 copy-start.3
  451.1 5.0 copy-start.4
  451.1 19.6 %reduce-scatter.27.cloned.1.call-start = ((), (), s32[]{:S(2)}) async-start(), calls=%async_computation.19 | async-start | bytes 98304 | tf_op jit(solution)/shard_map/reduce_scatter | solution.py:64
  453.6 25.0 %reduce-scatter.29.cloned.1.call-start = ((), (), s32[]{:S(2)}) async-start(), calls=%async_computation.20 | async-start | bytes 98304 | tf_op jit(solution)/shard_map/reduce_scatter | solution.py:67
  456.0 33.5 %reduce-scatter.33.cloned.1.call-start = ((), (), s32[]{:S(2)}) async-start(), calls=%async_computation.22 | async-start | bytes 98304 | tf_op jit(solution)/shard_map/reduce_scatter | solution.py:63
  458.1 42.1 %reduce-scatter.35.cloned.1.call-start = ((), (), s32[]{:S(2)}) async-start(), calls=%async_computation.23 | async-start | bytes 98304 | tf_op jit(solution)/shard_map/reduce_scatter | solution.py:68
  460.2 51.5 %reduce-scatter.31.cloned.1.call-start = ((), (), s32[]{:S(2)}) async-start(), calls=%async_computation.21 | async-start | bytes 98304 | tf_op jit(solution)/shard_map/reduce_scatter | solution.py:65
  462.3 409.6 %all-gather.7.cloned.1.call-start = ((), (), s32[]{:S(2)}) async-start(), calls=%async_computation.25 | async-start | bytes 35651584 | tf_op jit(solution)/shard_map/all_gather | solution.py:96
  511.7 3.2 copy-start
  522.2 1.6 copy-start.1
Sparse Core Ops, SparseCore 0:
  10.6 10.2 reduce-scatter.12
  23.1 8.6 reduce-scatter.14
  33.9 8.6 reduce-scatter.16
  45.3 8.6 reduce-scatter.18
  56.0 8.6 reduce-scatter.20
  66.7 8.6 reduce-scatter.22
  82.4 351.3 all-gather.4
  451.2 5.7 reduce-scatter.24
  459.2 8.6 reduce-scatter.26
  469.9 8.6 reduce-scatter.28
  480.8 8.6 reduce-scatter.32
  491.5 8.6 reduce-scatter.34
  503.0 8.6 reduce-scatter.30
  520.5 351.3 all-gather.6
